TPU v7x, 512 devices: a whole 4x4x16 slice. The times are simulated.
512 devices in a mesh: ep: 32 (over z, core), tp: 16 (over y, x).
Axes of the slice: x: 4, y: 4, z: 16, core: 2. Of those that a mesh axis runs over, the one named last changes fastest.
Arguments:
- queries: bfloat16 [16384, 1024], P('ep', 'tp'), may hold values from -9 to 9
- keys: bfloat16 [16384, 128], P('ep'), may hold values from -6 to 6
- values: bfloat16 [16384, 128], P('ep'), may hold values from -6 to 6
- sink_logits: float32 [16], P('tp'), may hold values from 2 to 7
- out_weight: bfloat16 [1024, 2048], P(None, 'tp'), may hold values from -0.8984375 to 0.8984375
- expert_input: bfloat16 [8192, 2048], P('ep'), may hold values from -6 to 6
- norm_gain: float32 [2048], replicated, may hold values from 0.1 to 1.9
- routes: int32 [8192, 2], P('ep'), may hold values from 0 to 31, all different within a row; in each aligned block of 256 rows (0 to 255, 256 to 511, ...) at most 32 rows name the same one
- route_weights: float32 [8192, 2], P('ep'), may hold values from 0.1 to 1
- gate_weight: bfloat16 [32, 2048, 4096], P('ep', None, 'tp'), may hold values from -0.125 to 0.125
- up_weight: bfloat16 [32, 2048, 4096], P('ep', None, 'tp'), may hold values from -0.125 to 0.125
- down_weight: bfloat16 [32, 4096, 2048], P('ep', 'tp'), may hold values from -0.09375 to 0.09375
Outputs:
- attn_out: bfloat16 [16384, 2048], P('ep', 'tp')
- expert_out: bfloat16 [8192, 2048], P('ep', 'tp')
Inputs may be any that keep to these rules, and one draw needn't show every extreme that they name: `routes`: each row names 2 different experts. Within the rows of one index of ep (aligned blocks of 256 rows) no expert is named by more than 32 rows, and in some blocks one expert is named by exactly 32 rows.
All inputs are finite; a program needn't handle non-finite values.
Results may differ from a plain program's by a relative error of at most 0.015.
Values may be sent and summed in bfloat16 or wider, within the bound.
A program may use at most 64 MiB of HBM per device.

v0:
```python
import jax
import jax.numpy as jnp
from jax import lax
from jax.sharding import Mesh
from jax.sharding import PartitionSpec as P

HEADS = 16
KV = 2
HD = 64
WINDOW = 128
TP = ("tp_0", "tp_1")


rms_eps = 1e-06
mask_value = -1e30


def passed_along(value, axis, steps):
    count = lax.axis_size(axis)
    first, last = (max(0, -steps), min(count, count - steps))
    return lax.ppermute(value, axis, [(source, source + steps) for source in range(first, last)])


def copy_for_each(x, axis):
    copies = jnp.broadcast_to(x, (lax.axis_size(axis), *x.shape))
    return lax.all_to_all(copies, axis, split_axis=0, concat_axis=0, tiled=True)


def joined_along(tiles, dim):
    dims = list(tiles.shape[1:])
    dims[dim] *= tiles.shape[0]
    return jnp.moveaxis(tiles, 0, dim).reshape(dims)


def gathered_copies(x, axis, dim):
    tiles = copy_for_each(x, axis)
    return joined_along(tiles, dim)


def own_rows(terms, axes):
    subtotal = terms.astype(jnp.bfloat16)
    for axis in axes:
        subtotal = lax.psum_scatter(subtotal, axis, scatter_dimension=0, tiled=True)
    return subtotal.astype(jnp.float32)


def rotate_heads(values_in, positions):
    half_dim = values_in.shape[-1] // 2
    inv_freq = 10000.0 ** (-jnp.arange(half_dim, dtype=jnp.float32) * (2.0 / values_in.shape[-1]))
    angles = positions[:, None] * inv_freq[None, :]
    cosine_table = jnp.cos(angles)[:, None, :]
    sine_table = jnp.sin(angles)[:, None, :]
    first_half = values_in[..., :half_dim]
    second_half = values_in[..., half_dim:]
    return jnp.concatenate(
        [
            first_half * cosine_table - second_half * sine_table,
            second_half * cosine_table + first_half * sine_table,
        ],
        axis=-1,
    )


def local(
    queries,
    keys,
    values,
    sink_logits,
    out_weight,
    expert_input,
    norm_gain,
    routes,
    route_weights,
    gate_weight,
    up_weight,
    down_weight,
):
    seq_rows = queries.shape[0]
    heads_here = queries.shape[1] // HD
    group_size = HEADS // KV
    kv_here = max(1, heads_here // group_size)
    heads_per_kv = heads_here // kv_here
    kv_first = lax.axis_index(TP) * heads_here // group_size
    key_local = lax.dynamic_slice_in_dim(keys, kv_first * HD, kv_here * HD, 1)
    value_local = lax.dynamic_slice_in_dim(values, kv_first * HD, kv_here * HD, 1)
    offset = lax.axis_index("ep") * seq_rows
    positions = (offset + jnp.arange(seq_rows, dtype=jnp.int32)).astype(jnp.float32)
    query_rot = rotate_heads(
        queries.astype(jnp.float32).reshape(seq_rows, heads_here, HD), positions
    ).astype(jnp.bfloat16)
    key_rot = rotate_heads(
        key_local.astype(jnp.float32).reshape(seq_rows, kv_here, HD), positions
    ).astype(jnp.bfloat16)
    value_heads = value_local.reshape(seq_rows, kv_here, HD)
    rim_pair = jnp.concatenate(
        [
            key_rot.reshape(seq_rows, kv_here * HD)[seq_rows - WINDOW :],
            value_local[seq_rows - WINDOW :],
        ],
        axis=1,
    )
    rim_pair = passed_along(rim_pair, "ep", 1)
    rim_key = rim_pair[:, : kv_here * HD].reshape(WINDOW, kv_here, HD)
    rim_value = rim_pair[:, kv_here * HD :].reshape(WINDOW, kv_here, HD)
    blocks = seq_rows // WINDOW

    def band_of(rim_part, local_part):
        padded = jnp.concatenate([rim_part, local_part], axis=0)
        earlier = padded[:seq_rows].reshape(blocks, WINDOW, kv_here, HD)
        current = padded[WINDOW:].reshape(blocks, WINDOW, kv_here, HD)
        return jnp.concatenate([earlier, current], axis=1)

    key_band = band_of(rim_key, key_rot)
    value_band = band_of(rim_value, value_heads)
    query_blocks = query_rot.reshape(blocks, WINDOW, kv_here, heads_per_kv, HD)
    scores = jnp.einsum(
        "nqhgd,nkhd->nhgqk", query_blocks, key_band, preferred_element_type=jnp.float32
    ) * HD ** (-0.5)
    block_start = offset + jnp.arange(blocks, dtype=jnp.int32)[:, None, None] * WINDOW
    query_pos = block_start + jnp.arange(WINDOW, dtype=jnp.int32)[None, :, None]
    key_pos = block_start - WINDOW + jnp.arange(2 * WINDOW, dtype=jnp.int32)[None, None, :]
    distance = query_pos - key_pos
    allowed = (distance >= 0) & (distance < WINDOW) & (key_pos >= 0)
    scores = jnp.where(allowed[:, None, None], scores, mask_value)
    sink_row = sink_logits.reshape(1, kv_here, heads_per_kv, 1)
    row_top = jnp.maximum(jnp.max(scores, axis=-1), sink_row)
    exp_scores = jnp.exp(scores - row_top[..., None])
    row_total = jnp.sum(exp_scores, axis=-1) + jnp.exp(sink_row - row_top)
    weights = (exp_scores / row_total[..., None]).astype(jnp.bfloat16)
    head_mix = jnp.einsum(
        "nhgqk,nkhd->nqhgd", weights, value_band, preferred_element_type=jnp.float32
    )
    head_mix = head_mix.astype(jnp.bfloat16).reshape(seq_rows, heads_here * HD)
    attn_out = jnp.dot(
        gathered_copies(head_mix, TP, 1), out_weight, preferred_element_type=jnp.float32
    ).astype(jnp.bfloat16)
    token_rows = expert_input.shape[0]
    top_count = routes.shape[1]
    expert_count = lax.axis_size("ep")
    capacity = 2 * top_count * token_rows // expert_count
    slot_total = expert_count * capacity
    input_wide = expert_input.astype(jnp.float32)
    inv_rms = lax.rsqrt(jnp.mean(input_wide * input_wide, axis=-1, keepdims=True) + rms_eps)
    normed = (input_wide * inv_rms * norm_gain[None, :]).astype(jnp.bfloat16)
    flat_expert = routes.reshape(-1)
    one_hot = (flat_expert[:, None] == jnp.arange(expert_count, dtype=jnp.int32)[None, :]).astype(
        jnp.int32
    )
    route_rank = jnp.sum(jnp.cumsum(one_hot, axis=0) * one_hot, axis=1) - 1
    slot_of_route = flat_expert * capacity + route_rank
    matches = slot_of_route[None, :] == jnp.arange(slot_total, dtype=jnp.int32)[:, None]
    route_token = jnp.arange(token_rows * top_count, dtype=jnp.int32) // top_count
    source_row = jnp.sum(jnp.where(matches, route_token[None, :] + 1, 0), axis=1) - 1
    occupied = source_row >= 0
    gate_local = gate_weight[0]
    up_local = up_weight[0]
    down_local = down_weight[0]
    column_count = normed.shape[1] // lax.axis_size(TP)
    own_columns = lax.dynamic_slice_in_dim(
        normed, lax.axis_index(TP) * column_count, column_count, 1
    )
    slot_rows = jnp.where(
        occupied[:, None],
        jnp.take(own_columns, jnp.maximum(source_row, 0), axis=0),
        jnp.zeros((), jnp.bfloat16),
    )
    outgoing = slot_rows.reshape(expert_count, capacity, column_count)
    arrived = lax.all_to_all(outgoing, "ep", split_axis=0, concat_axis=0, tiled=True)
    leading = arrived.shape[:2]
    portion = gathered_copies(arrived, TP, 2)
    flat_piece = portion.reshape(-1, portion.shape[2])
    gate_acc = jnp.dot(flat_piece, gate_local, preferred_element_type=jnp.float32)
    up_acc = jnp.dot(flat_piece, up_local, preferred_element_type=jnp.float32)
    hidden = (jax.nn.silu(gate_acc) * up_acc).astype(jnp.bfloat16)
    summed = own_rows(
        lax.dot_general(
            down_local, hidden, (((0,), (1,)), ((), ())), preferred_element_type=jnp.float32
        ),
        TP,
    )
    returned = summed.astype(jnp.bfloat16).reshape((summed.shape[0],) + leading)
    results_home = lax.all_to_all(returned, "ep", split_axis=1, concat_axis=1, tiled=True)
    home_flat = results_home.reshape(results_home.shape[0], -1)
    picked = jnp.take(home_flat, slot_of_route, axis=1).astype(jnp.float32)
    weighted = picked * route_weights.reshape(1, -1)
    combined = jnp.sum(weighted.reshape(results_home.shape[0], token_rows, top_count), axis=2)
    expert_out = combined.T.astype(jnp.bfloat16)
    return (attn_out, expert_out)


def solution(mesh):
    finer = Mesh(mesh.devices.reshape(mesh.shape["ep"], 4, 4), ("ep", "tp_0", "tp_1"))
    return jax.shard_map(
        local,
        mesh=finer,
        in_specs=(
            P("ep", TP),
            P("ep", None),
            P("ep", None),
            P(TP),
            P(None, TP),
            P("ep", None),
            P(),
            P("ep", None),
            P("ep", None),
            P("ep", None, TP),
            P("ep", None, TP),
            P("ep", TP, None),
        ),
        out_specs=(P("ep", TP), P("ep", TP)),
        check_vma=False,
    )
```

profile of v0, /device:TPU:1, one launch (start us, length us, event | category | flops | bytes accessed | tf_op | source)
XLA Modules:
  0.0 258.0 jit_solution(8480046307405987944)
XLA Ops:
  7.2 1.5 convert_element_type.84
  8.8 1.5 multiply_reduce_fusion
  10.7 1.2 reduce-window.6
  13.7 3.2 %gather_fusion = bf16[1024,128]{1,0:T(8,128)(2,1)S(1)} fusion(bf16[256,128]{1,0:T(8,128)(2,1)S(1)} %fusion.32, s32[1024]{0:T(1024)S(1)} %maximum_clamp_fusion), kind=kCustom, calls=%fused_computation | custom fusion | bytes 528384 | tf_op jit(solution)/shard_map/jit(_take)/gather | solution.py:164
  17.2 38.8 %all_to_all.20 = bf16[32,32,128]{2,1,0:T(8,128)(2,1)S(1)} all-to-all(bf16[32,32,128]{2,1,0:T(8,128)(2,1)S(1)} %select_select_fusion), channel_id=1, replica_groups=mesh['ep'=32,'tp_0'=4,'tp_1'=4] {'ep'}, dimensions={0} | all-to-all | bytes 524288 | tf_op jit(solution)/shard_map/all_to_all | solution.py:168
  56.8 56.3 %all_to_all.21 = bf16[16,32,32,128]{3,2,1,0:T(8,128)(2,1)S(1)} all-to-all(bf16[16,32,32,128]{3,2,1,0:T(8,128)(2,1)S(1)} %broadcast_in_dim.84), channel_id=1, replica_groups=mesh['ep'=32,'tp_0'=4,'tp_1'=4] {'tp_0','tp_1'}, dimensions={0} | all-to-all | bytes 8388608 | tf_op jit(solution)/shard_map/all_to_all | solution.py:26
  113.2 4.9 %copy.106 = bf16[32,32,16,128]{3,2,1,0:T(8,128)(2,1)S(1)} copy(bf16[32,32,16,128]{3,1,0,2:T(8,128)(2,1)S(1)} %bitcast.128) | data formatting | bytes 8388608 | tf_op jit(solution)/shard_map/transpose | solution.py:32
  118.0 2.0 copy-done.1
  120.0 1.3 fusion.2
  121.3 8.5 %convert_bitcast_fusion = bf16[2048,1024]{0,1:T(8,128)(2,1)} fusion(bf16[128,8,16,128]{3,2,1,0:T(8,128)(2,1)} %bitcast.131, bf16[1,256,2048]{2,1,0:T(8,128)(2,1)S(1)} %copy-done, bf16[1,2048,256]{2,1,0:T(8,128)(2,1)S(1)} %copy-done.9, f32[1024,256]{1,0:T(8,128)S(1)} %fusion.2), kind=kOutput, calls=%fused_computation.6 | convolution fusion | flops 2151153664 | bytes 11534336 | tf_op jit(solution)/shard_map/dot_general | solution.py:176
  129.8 0.8 copy-done.3
  131.5 3.3 %collective-permute-start = (bf16[128,128]{0,1:T(8,128)(2,1)S(1)}, bf16[128,128]{0,1:T(8,128)(2,1)S(1)}, u32[]{:S(2)}, u32[]{:S(2)}) collective-permute-start(bf16[128,128]{0,1:T(8,128)(2,1)S(1)} %pad_maximum_fusion.3), channel_id=1, source_target_pairs={{0,16},{16,32},{32,48},{48,64},{64,80},{80,96},{96,112},{112,128},... | collective-permute-start | bytes 98312 | tf_op jit(solution)/shard_map/ppermute | solution.py:21
  135.8 38.7 %reduce-scatter.5.cloned.1.call-done = bf16[512,1024]{0,1:T(8,128)(2,1)} async-done(((bf16[2048,1024]{0,1:T(8,128)(2,1)}), bf16[512,1024]{0,1:T(8,128)(2,1)}) %reduce-scatter.5.cloned.1.call-update) | async-done | bytes 1048592 | tf_op jit(solution)/shard_map/reduce_scatter | solution.py:43
  174.6 2.3 copy.110
  176.9 1.0 fusion.71
  178.4 1.1 broadcast_in_dim.76
  179.5 5.2 %all-to-all-start = ((bf16[16,512,64]{1,2,0:T(8,128)(2,1)}), bf16[16,512,64]{1,2,0:T(8,128)(2,1)S(1)}, u32[]{:S(2)}, u32[]{:S(2)}) async-start(bf16[16,512,64]{1,2,0:T(8,128)(2,1)} %broadcast_in_dim.76), calls=%async_computation | async-start | bytes 2097152 | tf_op jit(solution)/shard_map/all_to_all | solution.py:26
  184.7 25.0 %reduce-scatter.7.cloned.1.call-done = bf16[128,1024]{1,0:T(8,128)(2,1)} async-done(((bf16[512,1024]{1,0:T(8,128)(2,1)}), bf16[128,1024]{1,0:T(8,128)(2,1)}) %reduce-scatter.7.cloned.1.call-update) | async-done | bytes 262160
  209.7 1.8 copy.111
  211.5 14.0 %all-to-all-start.3 = ((bf16[128,32,32]{0,2,1:T(8,128)(2,1)}), bf16[128,32,32]{0,2,1:T(8,128)(2,1)S(1)}, u32[]{:S(2)}, u32[]{:S(2)}) async-start(bf16[128,32,32]{0,2,1:T(8,128)(2,1)} %bitcast.25), calls=%async_computation.4 | async-start | bytes 524288 | tf_op jit(solution)/shard_map/all_to_all | solution.py:182
  226.4 1.1 convolution_convert_fusion
  227.6 20.2 %all-to-all-done.3 = bf16[128,32,32]{0,2,1:T(8,128)(2,1)S(1)} async-done(((bf16[128,32,32]{0,2,1:T(8,128)(2,1)}), bf16[128,32,32]{0,2,1:T(8,128)(2,1)S(1)}, u32[]{:S(2)}, u32[]{:S(2)}) %all-to-all-start.3) | async-done | bytes 262176 | tf_op jit(solution)/shard_map/all_to_all | solution.py:182
  247.8 1.3 gather_fusion.1
  249.1 2.1 multiply_reduce_fusion.1
  (85 shorter events, 5.8 us)
Async XLA Ops:
  7.2 114.1 %copy-start = (bf16[1,256,2048]{2,1,0:T(8,128)(2,1)S(1)}, bf16[1,256,2048]{2,1,0:T(8,128)(2,1)}, u32[]{:S(2)}) copy-start(bf16[1,256,2048]{2,1,0:T(8,128)(2,1)} %param.23) | copy-start | bytes 3145732
  7.2 3.1 %copy-start.6 = (s32[256,2]{0,1:T(2,128)S(1)}, s32[256,2]{0,1:T(2,128)}, u32[]{:S(2)}) copy-start(s32[256,2]{0,1:T(2,128)} %param.19) | copy-start | bytes 6148
  7.2 167.4 %reduce-scatter.5.cloned.1.call-start = ((), (), s32[]{:S(2)}) async-start(), calls=%async_computation.6 | async-start | bytes 5242880 | tf_op jit(solution)/shard_map/reduce_scatter | solution.py:43
  113.2 6.8 %copy-start.8 = (bf16[1,2048,256]{2,1,0:T(8,128)(2,1)S(1)}, bf16[1,2048,256]{2,1,0:T(8,128)(2,1)}, u32[]{:S(2)}) copy-start(bf16[1,2048,256]{2,1,0:T(8,128)(2,1)} %param.21) | copy-start | bytes 3145732
  118.0 2.0 copy-start.1
  120.0 1.3 copy-start.9
  129.7 0.9 copy-start.3
  129.7 1.0 copy-start.4
  129.7 1.4 copy-start.5
  129.8 79.9 %reduce-scatter.7.cloned.1.call-start = ((), (), s32[]{:S(2)}) async-start(), calls=%async_computation.7 | async-start | bytes 1310720
  131.5 4.3 %collective-permute-start = (bf16[128,128]{0,1:T(8,128)(2,1)S(1)}, bf16[128,128]{0,1:T(8,128)(2,1)S(1)}, u32[]{:S(2)}, u32[]{:S(2)}) collective-permute-start(bf16[128,128]{0,1:T(8,128)(2,1)S(1)} %pad_maximum_fusion.3), channel_id=1, source_target_pairs={{0,16},{16,32},{32,48},{48,64},{64,80},{80,96},{96,112},{112,128},... | collective-permute-start | bytes 98312 | tf_op jit(solution)/shard_map/ppermute | solution.py:21
  177.9 48.3 %copy-start.7 = (f32[256,2]{0,1:T(2,128)S(1)}, f32[256,2]{0,1:T(2,128)}, u32[]{:S(2)}) copy-start(f32[256,2]{0,1:T(2,128)} %param.20) | copy-start | bytes 6148
  177.9 48.5 %copy-start.2 = (bf16[1024,128]{1,0:T(8,128)(2,1)S(1)}, bf16[1024,128]{1,0:T(8,128)(2,1)}, u32[]{:S(2)}) copy-start(bf16[1024,128]{1,0:T(8,128)(2,1)} %param.16) | copy-start | bytes 786436
  179.5 32.0 %all-to-all-start = ((bf16[16,512,64]{1,2,0:T(8,128)(2,1)}), bf16[16,512,64]{1,2,0:T(8,128)(2,1)S(1)}, u32[]{:S(2)}, u32[]{:S(2)}) async-start(bf16[16,512,64]{1,2,0:T(8,128)(2,1)} %broadcast_in_dim.76), calls=%async_computation | async-start | bytes 2097152 | tf_op jit(solution)/shard_map/all_to_all | solution.py:26
  211.5 36.3 %all-to-all-start.3 = ((bf16[128,32,32]{0,2,1:T(8,128)(2,1)}), bf16[128,32,32]{0,2,1:T(8,128)(2,1)S(1)}, u32[]{:S(2)}, u32[]{:S(2)}) async-start(bf16[128,32,32]{0,2,1:T(8,128)(2,1)} %bitcast.25), calls=%async_computation.4 | async-start | bytes 524288 | tf_op jit(solution)/shard_map/all_to_all | solution.py:182
Sparse Core Ops, SparseCore 0:
  129.9 44.6 reduce-scatter.4
  177.4 32.2 reduce-scatter.6
where the time goes:
time: 259 us; the launch traced here: 258 us
  blocking collectives  95.1 us (37%)
  waiting for transfers between devices  83.9 us (32%)
  starting transfers between devices  22.6 us (9%)
  local copies, waits for them, and re-layouts  21.1 us (8%)
  between operations  15.2 us (6%)
  matrix products  12.1 us (5%)
  other arithmetic  7.96 us (3%)
    all_to_all x1, blocking collectives, copy_for_each(): return lax.all_to_all(copies, axis, split_axis=0, concat_axis=0, tiled=True)  56.3 us
    all_to_all x1, blocking collectives, local(): lax.all_to_all(outgoing, 'ep', split_axis=0, concat_axis=0, tiled=True)  38.8 us
    reduce_scatter x1, waiting for transfers between devices, own_rows(): subtotal = lax.psum_scatter(subtotal, axis, scatter_dimension=0, tiled=True)  38.7 us
    unnamed x3, waiting for transfers between devices  25 us
    all_to_all x1, waiting for transfers between devices, local(): lax.all_to_all(returned, 'ep', split_axis=1, concat_axis=1, tiled=True)  20.2 us
    all_to_all x1, starting transfers between devices, local(): lax.all_to_all(returned, 'ep', split_axis=1, concat_axis=1, tiled=True)  14 us
    dot_general x1, matrix products, local(): lax.dot_general(down_local, hidden, (((0,), (1,)), ((), ())), preferred_e...  8.46 us
    unnamed x27, local copies, waits for them, and re-layouts  7.43 us
  transfers between devices with their start and end apart: 5, of which 3 were waited for; matrix products, arithmetic and copies ran while one was open for 3% of the time, Pallas kernels for 0%

commit v1 on v0

v1 whole, which is shorter than its diff:
```python
import functools

import jax
import jax.numpy as jnp
import numpy as np
from jax import lax
from jax.experimental import pallas as pl
from jax.experimental.pallas import tpu as pltpu
from jax.sharding import Mesh
from jax.sharding import PartitionSpec as P

HEADS = 16
KV = 2
HD = 64
WINDOW = 128
TP = ("tp_0", "tp_1")
NZ = 16
UNITS = 16
ATT_UNITS = 4
ALL_UNITS = UNITS + ATT_UNITS
SLOTS = 32
EXPERTS = 32
ROWS = 64
D = 2048
FF_HERE = 256
TOK_E = 256
TOK_A = 512
MESH = pl.DeviceIdType.MESH

AG3, AG4, MM, RS2, RS3, FIN = 2, 4, 6, 8, 10, 12

rms_eps = 1e-06
mask_value = -1e30

f32 = jnp.float32
bf16 = jnp.bfloat16


def unit_dz(u):
    j = u // 2
    dist = jnp.where(j < 4, 2 * j + 1, 16 - 2 * j)
    sign = 1 - 2 * (u % 2)
    return jnp.where(u == 9, 0, sign * dist)


def rope_tables():
    lane = np.arange(128) % 32
    freq = 10000.0 ** (-lane * (2.0 / HD))
    sign = np.where(np.arange(128) % 64 < 32, -1.0, 1.0)
    near = np.arange(WINDOW)[:, None] * freq[None, :]
    far = (np.arange(128) * WINDOW)[:, None] * freq[None, :]
    tables = np.stack([np.cos(near), np.sin(near) * sign, np.cos(far), np.sin(far) * sign])
    return tables.astype(np.float32)


def dot(a, b):
    return jnp.dot(a, b, preferred_element_type=f32)


def kernel(
    q_in, k_in, v_in, sink_ref, ow_in, x_in, gain_in, routes_in, rw_in, wg_in, wu_in, wd_in, trig_in,
    attn_ref, eout_ref,
    q_v, k_v, v_v, ow_v, x_v, gain_v, routes_v, rw_v, wg_v, wu_v, wd_v, trig_v,
    nrm, disp, w01, qp, kv, xg, yb, ra, rb, rc, tb, qb, rd, fb, home,
    in_sem, zs, zr, hs, hr, a1s, a1r, a3s, a3r, a4s, a4r, b1s, b1r, b2s, b2r, b3s, b3r, ks, kr,
):
    ep = lax.axis_index("ep")
    y = lax.axis_index("tp_0")
    x = lax.axis_index("tp_1")
    z = ep // 2
    core = ep % 2
    tp = y * 4 + x
    sg = 1 - 2 * core

    barrier = pltpu.get_barrier_semaphore()

    def hello(step, carry):
        pl.semaphore_signal(barrier, inc=1, device_id=((ep + step) % 32, y, x), device_id_type=MESH)
        return carry

    lax.fori_loop(1, 32, hello, 0)
    for k in (1, 2, 3):
        pl.semaphore_signal(barrier, inc=1, device_id=(ep, (y + k) % 4, x), device_id_type=MESH)
        pl.semaphore_signal(barrier, inc=1, device_id=(ep, y, (x + k) % 4), device_id_type=MESH)

    pairs = [
        (routes_in, routes_v), (x_in, x_v), (gain_in, gain_v), (rw_in, rw_v), (trig_in, trig_v), (q_in, q_v),
        (k_in, k_v), (v_in, v_v), (wg_in, wg_v), (wu_in, wu_v), (wd_in, wd_v), (ow_in, ow_v),
    ]
    loads = [pltpu.make_async_copy(a, b, in_sem.at[n]) for n, (a, b) in enumerate(pairs)]
    for load in loads:
        load.start()
    (l_routes, l_x, l_gain, l_rw, l_trig, l_q, l_k, l_v, l_wg, l_wu, l_wd, l_ow) = loads

    l_routes.wait()
    routes = routes_v[...]
    e_iota = lax.broadcasted_iota(jnp.int32, (TOK_E, EXPERTS), 1)
    one0 = (routes[:, 0:1] == e_iota).astype(f32)
    one1 = (routes[:, 1:2] == e_iota).astype(f32)
    t_row = lax.broadcasted_iota(jnp.int32, (TOK_E, TOK_E), 0)
    t_col = lax.broadcasted_iota(jnp.int32, (TOK_E, TOK_E), 1)
    lower = (t_col < t_row).astype(f32).astype(bf16)
    rank = dot(lower, (one0 + one1).astype(bf16))
    rank0 = jnp.sum(one0 * rank, axis=1, keepdims=True)
    rank1 = jnp.sum(one1 * rank, axis=1, keepdims=True)
    eye = (t_col == t_row).astype(f32)
    ones = jnp.ones((16, TOK_E), bf16)

    def as_row(column):
        return dot(ones, (eye * column).astype(bf16))[0:1, :]

    slot_row0 = as_row(routes[:, 0:1].astype(f32)) * float(SLOTS) + as_row(rank0)
    slot_row1 = as_row(routes[:, 1:2].astype(f32)) * float(SLOTS) + as_row(rank1)

    l_x.wait()
    l_gain.wait()
    own_cols = pl.ds(pl.multiple_of(tp * 128, 128), 128)
    gain = gain_v[:, own_cols]

    def norm_rows(n, carry):
        rows = pl.ds(pl.multiple_of(n * 32, 32), 32)
        wide = x_v[rows, :].astype(f32)
        inv = lax.rsqrt(jnp.mean(wide * wide, axis=1, keepdims=True) + rms_eps)
        nrm[rows, :] = (x_v[rows, own_cols].astype(f32) * inv * gain).astype(bf16)
        return carry

    lax.fori_loop(0, 8, norm_rows, 0)
    normed = nrm[...]

    def fill_slots(n, carry):
        slot = (lax.broadcasted_iota(jnp.int32, (256, TOK_E), 0) + n * 256).astype(f32)
        pick = ((slot == slot_row0) | (slot == slot_row1)).astype(f32).astype(bf16)
        disp[pl.ds(n * 8, 8)] = dot(pick, normed).astype(bf16).reshape(8, SLOTS, 128)
        return carry

    lax.fori_loop(0, 4, fill_slots, 0)
    pl.semaphore_wait(barrier, 37)

    def place(u):
        odd = u % 2
        return jnp.where(odd == 1, x, y), jnp.where(odd == 1, y, x)

    def along_j(u, k):
        odd = u % 2
        return (ep, jnp.where(odd == 1, (y + k) % 4, y), jnp.where(odd == 1, x, (x + k) % 4))

    def along_i(u, k):
        odd = u % 2
        return (ep, jnp.where(odd == 1, y, (y + k) % 4), jnp.where(odd == 1, (x + k) % 4, x))

    fw = sg + 4
    bw = 4 - sg

    def z_copy(u, cc):
        dest = ((z - unit_dz(u) + NZ) % NZ) * 2 + cc
        i, j = place(u)
        return pltpu.make_async_remote_copy(
            src_ref=disp.at[dest], dst_ref=xg.at[u, i, j, core],
            send_sem=zs.at[u, cc], recv_sem=zr.at[u, core],
            device_id=(dest, y, x), device_id_type=MESH,
        )

    def z_wait(u, c):
        i, j = place(u)
        pltpu.make_async_remote_copy(
            src_ref=disp.at[0], dst_ref=xg.at[u, i, j, c],
            send_sem=zs.at[u, c], recv_sem=zr.at[u, c],
            device_id=(ep ^ 1, y, x), device_id_type=MESH,
        ).wait_recv()

    def z_send(u, carry):
        for cc in (0, 1):
            @pl.when(jnp.logical_not((u == 9) & (core == cc)))
            def _():
                z_copy(u, cc).start()
        return carry

    lax.fori_loop(0, UNITS, z_send, 0)
    xg[9, x, y, core] = disp[ep]

    l_trig.wait()
    l_q.wait()
    l_k.wait()
    l_v.wait()
    group = y // 2
    lane = lax.broadcasted_iota(jnp.int32, (WINDOW, 128), 1)
    first = lane < HD

    def rotate_block(n, carry):
        rows = pl.ds(pl.multiple_of(n * WINDOW, WINDOW), WINDOW)
        q = q_v[rows, :].astype(f32)
        k = k_v[rows, :].astype(f32)
        v = v_v[rows, :].astype(f32)
        k = jnp.where(group == 0, pltpu.roll(k, HD, 1), k)
        v = jnp.where(group == 0, pltpu.roll(v, HD, 1), v)
        both = jnp.where(first, jnp.concatenate([q, q], axis=1), k)
        block = ep * 4 + n
        cb = trig_v[2, pl.ds(block, 1), :]
        sb = trig_v[3, pl.ds(block, 1), :]
        cr = trig_v[0]
        sr = trig_v[1]
        cos = cb * cr - sb * sr
        sin = sb * cr + cb * sr
        swapped = jnp.where(lane % HD < HD // 2, pltpu.roll(both, 128 - HD // 2, 1), pltpu.roll(both, HD // 2, 1))
        turned = both * cos + swapped * sin
        qp[n] = jnp.where(first, turned, 0.0).astype(bf16)
        kv[n + 1] = jnp.where(first, pltpu.roll(turned, HD, 1), v).astype(bf16)
        return carry

    lax.fori_loop(0, 4, rotate_block, 0)
    rim = pltpu.make_async_remote_copy(
        src_ref=kv.at[4], dst_ref=kv.at[0], send_sem=ks.at[0], recv_sem=kr.at[0],
        device_id=((ep + 1) % 32, y, x), device_id_type=MESH,
    )
    rim.start()

    l_ow.wait()

    def spread(h, carry):
        w = ow_v[pl.ds(pl.multiple_of(h * HD, HD), HD), :]
        zero = jnp.zeros((HD, 128), bf16)
        w01[pl.ds(pl.multiple_of(h * 128, 128), HD), :] = jnp.concatenate([w, zero], axis=1)
        w01[pl.ds(pl.multiple_of(h * 128 + HD, HD), HD), :] = jnp.concatenate([zero, w], axis=1)
        return carry

    lax.fori_loop(0, HEADS, spread, 0)

    sink = sink_ref[0]
    q_pos = lax.broadcasted_iota(jnp.int32, (WINDOW, 2 * WINDOW), 0) + WINDOW
    k_pos = lax.broadcasted_iota(jnp.int32, (WINDOW, 2 * WINDOW), 1)
    banded = (q_pos >= k_pos) & (q_pos - k_pos < WINDOW)

    def mix_of(n):
        keys = kv[pl.ds(n, 2)].reshape(2 * WINDOW, 128)
        scores = lax.dot_general(qp[n], keys, (((1,), (1,)), ((), ())), preferred_element_type=f32) * HD ** (-0.5)
        allowed = banded & ((ep * 4 + n) * WINDOW + k_pos >= WINDOW)
        scores = jnp.where(allowed, scores, mask_value)
        top = jnp.maximum(jnp.max(scores, axis=1, keepdims=True), sink)
        e = jnp.exp(scores - top)
        total = jnp.sum(e, axis=1, keepdims=True) + jnp.exp(sink - top)
        return dot((e / total).astype(bf16), keys)

    def attend(n):
        mixed = jnp.where(first, pltpu.roll(mix_of(n), HD, 1), mix_of(n + 2)).astype(bf16)
        xg[UNITS + 2 * n, y, x] = mixed[:ROWS].reshape(2, SLOTS, 128)
        xg[UNITS + 2 * n + 1, x, y] = mixed[ROWS:].reshape(2, SLOTS, 128)

    def ag1_copy(u, k):
        i, j = place(u)
        return pltpu.make_async_remote_copy(
            src_ref=xg.at[u, i, j], dst_ref=xg.at[u, i, j],
            send_sem=a1s.at[u, k - 1], recv_sem=a1r.at[u, k - 1],
            device_id=along_j(u, k), device_id_type=MESH,
        )

    def ag3_copy(u, side):
        i, j = place(u)
        return pltpu.make_async_remote_copy(
            src_ref=xg.at[u, i], dst_ref=xg.at[u, i],
            send_sem=a3s.at[u, side], recv_sem=a3r.at[u, side],
            device_id=along_i(u, bw if side else fw), device_id_type=MESH,
        )

    def ag4_copy(u):
        i, j = place(u)
        row = (i + bw) % 4
        return pltpu.make_async_remote_copy(
            src_ref=xg.at[u, row], dst_ref=xg.at[u, row],
            send_sem=a4s.at[u], recv_sem=a4r.at[u],
            device_id=along_i(u, fw), device_id_type=MESH,
        )

    def got(copy_like, dst, sem):
        pltpu.make_async_remote_copy(
            src_ref=dst, dst_ref=dst, send_sem=copy_like, recv_sem=sem,
            device_id=(ep ^ 1, y, x), device_id_type=MESH,
        ).wait_recv()

    def ag1_got(u, k):
        i, j = place(u)
        got(a1s.at[u, k - 1], xg.at[u, i, (j + 4 - k) % 4], a1r.at[u, k - 1])

    def ag3_got(u, side):
        i, j = place(u)
        got(a3s.at[u, side], xg.at[u, (i + (fw if side else bw)) % 4], a3r.at[u, side])

    def ag4_got(u):
        i, j = place(u)
        got(a4s.at[u], xg.at[u, (i + 2) % 4], a4r.at[u])

    def gathered(u):
        odd = u % 2
        tiles = []
        for yy in range(4):
            for xx in range(4):
                a = jnp.where(odd == 1, xx, yy)
                b = jnp.where(odd == 1, yy, xx)
                tiles.append(xg[u, a, b].reshape(ROWS, 128))
        return jnp.concatenate(tiles, axis=1)

    def rs1_copy(u, side):
        i, j = place(u)
        dest = (j + (bw if side else 2)) % 4
        return pltpu.make_async_remote_copy(
            src_ref=yb.at[u, dest], dst_ref=(rb if side else ra).at[u],
            send_sem=b1s.at[u, side], recv_sem=b1r.at[u, side],
            device_id=along_j(u, bw if side else fw), device_id_type=MESH,
        )

    def rs2_copy(u):
        return pltpu.make_async_remote_copy(
            src_ref=tb.at[u], dst_ref=rc.at[u], send_sem=b2s.at[u], recv_sem=b2r.at[u],
            device_id=along_j(u, fw), device_id_type=MESH,
        )

    def rs3_copy(u, k):
        i, j = place(u)
        return pltpu.make_async_remote_copy(
            src_ref=qb.at[u, (i + k) % 4], dst_ref=rd.at[u, k - 1],
            send_sem=b3s.at[u, k - 1], recv_sem=b3r.at[u, k - 1],
            device_id=along_i(u, k), device_id_type=MESH,
        )

    def home_copy(u, cc):
        dest = ((z + unit_dz(u) + NZ) % NZ) * 2 + cc
        return pltpu.make_async_remote_copy(
            src_ref=fb.at[u, cc], dst_ref=home.at[ep],
            send_sem=hs.at[u, cc], recv_sem=hr.at[u, core],
            device_id=(dest, y, x), device_id_type=MESH,
        )

    def not_own(u, cc):
        return jnp.logical_not((u == 9) & (core == cc))

    def tick(t, carry):
        u1 = t

        @pl.when(t == 2)
        def _():
            rim.wait_recv()
            attend(0)

        @pl.when(t == 4)
        def _():
            attend(1)

        @pl.when(u1 < ALL_UNITS)
        def _():
            @pl.when(u1 < UNITS)
            def _():
                for c in (0, 1):
                    @pl.when(not_own(u1, c))
                    def _():
                        z_wait(u1, c)
            for k in (1, 2, 3):
                ag1_copy(u1, k).start()

        u2 = t - RS2

        @pl.when((u2 >= 0) & (u2 < UNITS))
        def _():
            i, j = place(u2)
            rs = rs1_copy(u2, 0)
            rs.wait_recv()
            tb[u2] = (ra[u2].astype(f32) + yb[u2, (j + fw) % 4].astype(f32)).astype(bf16)
            rs2_copy(u2).start()

        u3 = t - AG3

        @pl.when((u3 >= 0) & (u3 < ALL_UNITS))
        def _():
            for k in (1, 2, 3):
                ag1_got(u3, k)
            ag3_copy(u3, 0).start()
            ag3_copy(u3, 1).start()

        u4 = t - AG4

        @pl.when((u4 >= 0) & (u4 < ALL_UNITS))
        def _():
            ag3_got(u4, 0)
            ag4_copy(u4).start()

        u5 = t - RS3

        @pl.when((u5 >= 0) & (u5 < UNITS))
        def _():
            i, j = place(u5)
            rs1_copy(u5, 1).wait_recv()
            rs2_copy(u5).wait_recv()
            qb[u5] = (yb[u5, j].astype(f32) + rc[u5].astype(f32) + rb[u5].astype(f32)).astype(bf16)
            for k in (1, 2, 3):
                rs3_copy(u5, k).start()

        u6 = t - FIN

        @pl.when((u6 >= 0) & (u6 < UNITS))
        def _():
            i, j = place(u6)
            for k in (1, 2, 3):
                rs3_copy(u6, k).wait_recv()
            total = qb[u6, i].astype(f32) + rd[u6, 0].astype(f32) + rd[u6, 1].astype(f32) + rd[u6, 2].astype(f32)
            fb[u6] = total.astype(bf16).reshape(2, SLOTS, 128)
            for cc in (0, 1):
                @pl.when(not_own(u6, cc))
                def _():
                    home_copy(u6, cc).start()

                @pl.when(jnp.logical_not(not_own(u6, cc)))
                def _():
                    home[ep] = fb[u6, cc]

        um = t - MM

        @pl.when(um == 0)
        def _():
            l_wg.wait()
            l_wu.wait()
            l_wd.wait()

        @pl.when((um >= 0) & (um < ALL_UNITS))
        def _():
            ag3_got(um, 1)
            ag4_got(um)

        @pl.when((um >= 0) & (um < UNITS))
        def _():
            i, j = place(um)
            odd = um % 2
            rows_in = gathered(um)
            gate = dot(rows_in, wg_v[...])
            up = dot(rows_in, wu_v[...])
            hidden = (gate / (1.0 + jnp.exp(-gate)) * up).astype(bf16)
            for yy in range(4):
                part = dot(hidden, wd_v[:, yy * 512:(yy + 1) * 512]).astype(bf16)
                for xx in range(4):
                    a = jnp.where(odd == 1, yy, xx)
                    b = jnp.where(odd == 1, xx, yy)
                    yb[um, a, b] = part[:, xx * 128:(xx + 1) * 128]
            rs1_copy(um, 0).start()
            rs1_copy(um, 1).start()

        @pl.when((um >= UNITS) & (um < ALL_UNITS))
        def _():
            out = dot(gathered(um), w01[...]).astype(bf16)
            row = (um - UNITS) * ROWS
            attn_ref[pl.ds(pl.multiple_of(row, ROWS), ROWS), :] = out[:, :128]
            attn_ref[pl.ds(pl.multiple_of(row + 256, ROWS), ROWS), :] = out[:, 128:]

        @pl.when((u6 >= 0) & (u6 < ALL_UNITS))
        def _():
            for k in (1, 2, 3):
                ag1_copy(u6, k).wait_send()
            ag3_copy(u6, 0).wait_send()
            ag3_copy(u6, 1).wait_send()
            ag4_copy(u6).wait_send()

        @pl.when((u6 >= 0) & (u6 < UNITS))
        def _():
            for cc in (0, 1):
                @pl.when(not_own(u6, cc))
                def _():
                    z_copy(u6, cc).wait_send()
            rs1_copy(u6, 0).wait_send()
            rs1_copy(u6, 1).wait_send()
            rs2_copy(u6).wait_send()
            for k in (1, 2, 3):
                rs3_copy(u6, k).wait_send()

        return carry

    lax.fori_loop(0, ALL_UNITS + FIN, tick, 0)

    l_rw.wait()
    weights = rw_v[...]
    slot0 = jnp.sum(one0 * (rank + e_iota.astype(f32) * float(SLOTS)), axis=1, keepdims=True)
    slot1 = jnp.sum(one1 * (rank + e_iota.astype(f32) * float(SLOTS)), axis=1, keepdims=True)
    slot_lane = lax.broadcasted_iota(jnp.int32, (TOK_E, EXPERTS * SLOTS), 1).astype(f32)
    pick0 = (slot_lane == slot0).astype(f32).astype(bf16)
    pick1 = (slot_lane == slot1).astype(f32).astype(bf16)

    def arrived(u, carry):
        for c in (0, 1):
            @pl.when(not_own(u, c))
            def _():
                src = ((z - unit_dz(u) + NZ) % NZ) * 2 + c
                got(hs.at[u, c], home.at[src], hr.at[u, c])
                home_copy(u, c).wait_send()
        return carry

    lax.fori_loop(0, UNITS, arrived, 0)
    rim.wait_send()
    results = home[...].reshape(EXPERTS * SLOTS, 128)
    combined = dot(pick0, results) * weights[:, 0:1] + dot(pick1, results) * weights[:, 1:2]
    eout_ref[...] = combined.astype(bf16)


def local(
    queries,
    keys,
    values,
    sink_logits,
    out_weight,
    expert_input,
    norm_gain,
    routes,
    route_weights,
    gate_weight,
    up_weight,
    down_weight,
):
    any_spec = pl.BlockSpec(memory_space=pl.ANY)
    vmem = pl.BlockSpec(memory_space=pltpu.VMEM)
    smem = pl.BlockSpec(memory_space=pltpu.SMEM)
    dma = pltpu.SemaphoreType.DMA
    trig = jnp.asarray(rope_tables())
    return pl.pallas_call(
        kernel,
        out_shape=(
            jax.ShapeDtypeStruct((TOK_A, 128), bf16),
            jax.ShapeDtypeStruct((TOK_E, 128), bf16),
        ),
        in_specs=[any_spec] * 3 + [smem] + [any_spec] * 9,
        out_specs=(vmem, vmem),
        scratch_shapes=[
            pltpu.VMEM((TOK_A, HD), bf16),
            pltpu.VMEM((TOK_A, 128), bf16),
            pltpu.VMEM((TOK_A, 128), bf16),
            pltpu.VMEM((HEADS * HD, 128), bf16),
            pltpu.VMEM((TOK_E, D), bf16),
            pltpu.VMEM((1, D), f32),
            pltpu.VMEM((TOK_E, 2), jnp.int32),
            pltpu.VMEM((TOK_E, 2), f32),
            pltpu.VMEM((D, FF_HERE), bf16),
            pltpu.VMEM((D, FF_HERE), bf16),
            pltpu.VMEM((FF_HERE, D), bf16),
            pltpu.VMEM((4, 128, 128), f32),
            pltpu.VMEM((TOK_E, 128), bf16),
            pltpu.VMEM((EXPERTS, SLOTS, 128), bf16),
            pltpu.VMEM((D, 256), bf16),
            pltpu.VMEM((4, WINDOW, 128), bf16),
            pltpu.VMEM((5, WINDOW, 128), bf16),
            pltpu.VMEM((ALL_UNITS, 4, 4, 2, SLOTS, 128), bf16),
            pltpu.VMEM((UNITS, 4, 4, ROWS, 128), bf16),
            pltpu.VMEM((UNITS, 4, ROWS, 128), bf16),
            pltpu.VMEM((UNITS, 4, ROWS, 128), bf16),
            pltpu.VMEM((UNITS, 4, ROWS, 128), bf16),
            pltpu.VMEM((UNITS, 4, ROWS, 128), bf16),
            pltpu.VMEM((UNITS, 4, ROWS, 128), bf16),
            pltpu.VMEM((UNITS, 3, ROWS, 128), bf16),
            pltpu.VMEM((UNITS, 2, SLOTS, 128), bf16),
            pltpu.VMEM((EXPERTS, SLOTS, 128), bf16),
            dma((12,)),
            dma((UNITS, 2)),
            dma((UNITS, 2)),
            dma((UNITS, 2)),
            dma((UNITS, 2)),
            dma((ALL_UNITS, 3)),
            dma((ALL_UNITS, 3)),
            dma((ALL_UNITS, 2)),
            dma((ALL_UNITS, 2)),
            dma((ALL_UNITS,)),
            dma((ALL_UNITS,)),
            dma((UNITS, 2)),
            dma((UNITS, 2)),
            dma((UNITS,)),
            dma((UNITS,)),
            dma((UNITS, 3)),
            dma((UNITS, 3)),
            dma((1,)),
            dma((1,)),
        ],
        compiler_params=pltpu.CompilerParams(
            collective_id=0, has_side_effects=True, vmem_limit_bytes=60 * 1024 * 1024
        ),
    )(
        queries, keys, values, sink_logits, out_weight, expert_input, norm_gain.reshape(1, D), routes, route_weights,
        gate_weight[0], up_weight[0], down_weight[0], trig,
    )


def solution(mesh):
    finer = Mesh(mesh.devices.reshape(mesh.shape["ep"], 4, 4), ("ep", "tp_0", "tp_1"))
    return jax.shard_map(
        local,
        mesh=finer,
        in_specs=(
            P("ep", TP),
            P("ep", None),
            P("ep", None),
            P(TP),
            P(None, TP),
            P("ep", None),
            P(),
            P("ep", None),
            P("ep", None),
            P("ep", None, TP),
            P("ep", None, TP),
            P("ep", TP, None),
        ),
        out_specs=(P("ep", TP), P("ep", TP)),
        check_vma=False,
    )
```

time: 259 us -> 109 us (0.42)
  Pallas kernels: 0 us -> 102 us
  blocking collectives: 95.1 us -> 0 us
  waiting for transfers between devices: 83.9 us -> 0 us
  starting transfers between devices: 22.6 us -> 0 us
  local copies, waits for them, and re-layouts: 21.1 us -> 5.41 us
  between operations: 15.2 us -> 1.3 us
  matrix products: 12.1 us -> 0 us
  other arithmetic: 7.96 us -> 0 us
    pallas_call x0 -> x1, Pallas kernels: none -> 102 us  [local(): pl.pallas_call(kernel, out_shape=(jax.ShapeDtypeStruct((TOK_A, 128), bf16...]
    all_to_all x2 -> x0, blocking collectives: 95.1 us -> none  [the longest x1 56.3 us: copy_for_each(): return lax.all_to_all(copies, axis, split_axis=0, concat_axis=0, tiled=True)]
    reduce_scatter x1 -> x0, waiting for transfers between devices: 38.7 us -> none  [own_rows(): subtotal = lax.psum_scatter(subtotal, axis, scatter_dimension=0, tiled=True)]
    unnamed x3 -> x0, waiting for transfers between devices: 25 us -> none
    all_to_all x2 -> x0, waiting for transfers between devices: 20.2 us -> none  [the longest x1 20.2 us: local(): lax.all_to_all(returned, 'ep', split_axis=1, concat_axis=1, tiled=True)]
    all_to_all x2 -> x0, starting transfers between devices: 19.2 us -> none  [the longest x1 14 us: local(): lax.all_to_all(returned, 'ep', split_axis=1, concat_axis=1, tiled=True)]
    dot_general x5 -> x0, matrix products: 12.1 us -> none  [the longest x1 8.46 us: local(): lax.dot_general(down_local, hidden, (((0,), (1,)), ((), ())), preferred_e...]
    transpose x1 -> x0, local copies, waits for them, and re-layouts: 4.86 us -> none  [joined_along(): return jnp.moveaxis(tiles, 0, dim).reshape(dims)]
  transfers between devices with their start and end apart: 5 -> 0, of which waited for: 3 -> 0; matrix products, arithmetic and copies ran while one was open for 3% -> 0% of each run, Pallas kernels for 0% -> 0%
where the time goes in v1:
time: 109 us
  Pallas kernels  102 us (94%)
  local copies, waits for them, and re-layouts  5.41 us (5%)
  between operations  1.3 us (1%)
    pallas_call x1, Pallas kernels, local(): pl.pallas_call(kernel, out_shape=(jax.ShapeDtypeStruct((TOK_A, 128), bf16...  102 us
    unnamed x11, local copies, waits for them, and re-layouts  5.41 us

profile of v1, /device:TPU:1, one launch (start us, length us, event | category | flops | bytes accessed | tf_op | source)
XLA Modules:
  0.0 108.8 jit_solution(9539028100326394534)
XLA Ops:
  1.3 0.0 copy-start.1
  1.3 1.6 %copy.15.q_in = bf16[512,64]{1,0:T(8,128)(2,1)} copy(bf16[512,64]{0,1:T(8,128)(2,1)} %param.13) | data formatting | bytes 131072 | tf_op args[0]
  2.9 0.0 copy-done.1
  2.9 0.0 copy-start.2
  2.9 0.8 copy.16.routes_in
  3.7 0.0 copy-done.2
  3.7 0.8 copy.17.rw_in
  4.5 102.0 %shard_map.140 = (bf16[512,128]{1,0:T(8,128)(2,1)}, bf16[256,128]{1,0:T(8,128)(2,1)}) custom-call(bf16[512,64]{1,0:T(8,128)(2,1)} %copy.15.q_in, bf16[512,128]{1,0:T(8,128)(2,1)} %k_in.1, bf16[512,128]{1,0:T(8,128)(2,1)} %v_in.1, f32[1]{0:T(128)S(6)} %copy.20.sink_ref, bf16[1024,128]{1,0:T(8,128)(2,1)} %ow_in.1, bf16[256,2048]{1,0:T(8,128)(2,1)} %x_in.1, ...), custom_call_target="tpu_custom_call" | custom-call | tf_op jit(solution)/shard_map/pallas_call | solution.py:517
  106.5 0.0 copy-start
  106.5 1.6 %copy.21 = bf16[512,128]{1,0:T(8,128)(2,1)} copy(bf16[512,128]{1,0:T(8,128)(2,1)} %get-tuple-element.4) | data formatting | bytes 262144
  108.1 0.0 copy-done
  108.1 0.6 copy.22
Async XLA Ops:
  1.3 1.6 %copy-start.1 = (s32[256,2]{0,1:T(2,128)S(1)}, s32[256,2]{0,1:T(2,128)}, u32[]{:S(2)}) copy-start(s32[256,2]{0,1:T(2,128)} %param.20) | copy-start | bytes 6148
  2.9 0.8 copy-start.2
  106.5 1.6 %copy-start = (bf16[256,128]{1,0:T(8,128)(2,1)S(1)}, bf16[256,128]{1,0:T(8,128)(2,1)}, u32[]{:S(2)}) copy-start(bf16[256,128]{1,0:T(8,128)(2,1)} %get-tuple-element.5) | copy-start | bytes 196612

commit v2 on v1

--- a/solution.py
+++ b/solution.py
@@ -1,5 +1,3 @@
-import functools
-
 import jax
 import jax.numpy as jnp
 import numpy as np
@@ -26,6 +24,8 @@
 TOK_E = 256
 TOK_A = 512
 MESH = pl.DeviceIdType.MESH
+OWN = 15
+ATTEND = (8, 10)
 
 AG3, AG4, MM, RS2, RS3, FIN = 2, 4, 6, 8, 10, 12
 
@@ -37,10 +37,10 @@
 
 
 def unit_dz(u):
-    j = u // 2
-    dist = jnp.where(j < 4, 2 * j + 1, 16 - 2 * j)
-    sign = 1 - 2 * (u % 2)
-    return jnp.where(u == 9, 0, sign * dist)
+    late = u - 7
+    out = jnp.where(u == 6, 8, (2 + 2 * (u // 2)) * (1 - 2 * (u % 2)))
+    back = jnp.where(u == OWN, 0, (7 - 2 * (late // 2)) * (1 - 2 * (late % 2)))
+    return jnp.where(u < 7, out, back)
 
 
 def rope_tables():
@@ -62,7 +62,7 @@
     attn_ref, eout_ref,
     q_v, k_v, v_v, ow_v, x_v, gain_v, routes_v, rw_v, wg_v, wu_v, wd_v, trig_v,
     nrm, disp, w01, qp, kv, xg, yb, ra, rb, rc, tb, qb, rd, fb, home,
-    in_sem, zs, zr, hs, hr, a1s, a1r, a3s, a3r, a4s, a4r, b1s, b1r, b2s, b2r, b3s, b3r, ks, kr,
+    in_sem, zs, zr, hs, hr, ags, a1r, a3r, a4r, rss, b1r, b2r, b3r, rims, rimr,
 ):
     ep = lax.axis_index("ep")
     y = lax.axis_index("tp_0")
@@ -72,17 +72,6 @@
     tp = y * 4 + x
     sg = 1 - 2 * core
 
-    barrier = pltpu.get_barrier_semaphore()
-
-    def hello(step, carry):
-        pl.semaphore_signal(barrier, inc=1, device_id=((ep + step) % 32, y, x), device_id_type=MESH)
-        return carry
-
-    lax.fori_loop(1, 32, hello, 0)
-    for k in (1, 2, 3):
-        pl.semaphore_signal(barrier, inc=1, device_id=(ep, (y + k) % 4, x), device_id_type=MESH)
-        pl.semaphore_signal(barrier, inc=1, device_id=(ep, y, (x + k) % 4), device_id_type=MESH)
-
     pairs = [
         (routes_in, routes_v), (x_in, x_v), (gain_in, gain_v), (rw_in, rw_v), (trig_in, trig_v), (q_in, q_v),
         (k_in, k_v), (v_in, v_v), (wg_in, wg_v), (wu_in, wu_v), (wd_in, wd_v), (ow_in, ow_v),
@@ -92,25 +81,27 @@
         load.start()
     (l_routes, l_x, l_gain, l_rw, l_trig, l_q, l_k, l_v, l_wg, l_wu, l_wd, l_ow) = loads
 
+    barrier = pltpu.get_barrier_semaphore()
+
+    def hello(step, carry):
+        pl.semaphore_signal(barrier, inc=1, device_id=((ep + step) % 32, y, x), device_id_type=MESH)
+        return carry
+
+    lax.fori_loop(1, 32, hello, 0)
+    for k in (1, 2, 3):
+        pl.semaphore_signal(barrier, inc=1, device_id=(ep, (y + k) % 4, x), device_id_type=MESH)
+        pl.semaphore_signal(barrier, inc=1, device_id=(ep, y, (x + k) % 4), device_id_type=MESH)
+
     l_routes.wait()
-    routes = routes_v[...]
-    e_iota = lax.broadcasted_iota(jnp.int32, (TOK_E, EXPERTS), 1)
-    one0 = (routes[:, 0:1] == e_iota).astype(f32)
-    one1 = (routes[:, 1:2] == e_iota).astype(f32)
+    e_iota = lax.broadcasted_iota(jnp.int32, (EXPERTS, TOK_E), 0)
+    one0 = (routes_v[0:1, :] == e_iota).astype(f32)
+    one1 = (routes_v[1:2, :] == e_iota).astype(f32)
     t_row = lax.broadcasted_iota(jnp.int32, (TOK_E, TOK_E), 0)
     t_col = lax.broadcasted_iota(jnp.int32, (TOK_E, TOK_E), 1)
-    lower = (t_col < t_row).astype(f32).astype(bf16)
-    rank = dot(lower, (one0 + one1).astype(bf16))
-    rank0 = jnp.sum(one0 * rank, axis=1, keepdims=True)
-    rank1 = jnp.sum(one1 * rank, axis=1, keepdims=True)
-    eye = (t_col == t_row).astype(f32)
-    ones = jnp.ones((16, TOK_E), bf16)
-
-    def as_row(column):
-        return dot(ones, (eye * column).astype(bf16))[0:1, :]
-
-    slot_row0 = as_row(routes[:, 0:1].astype(f32)) * float(SLOTS) + as_row(rank0)
-    slot_row1 = as_row(routes[:, 1:2].astype(f32)) * float(SLOTS) + as_row(rank1)
+    before = (t_row < t_col).astype(f32).astype(bf16)
+    place_of = dot((one0 + one1).astype(bf16), before) + (e_iota * SLOTS).astype(f32)
+    slot_row0 = jnp.sum(one0 * place_of, axis=0, keepdims=True)
+    slot_row1 = jnp.sum(one1 * place_of, axis=0, keepdims=True)
 
     l_x.wait()
     l_gain.wait()
@@ -151,32 +142,47 @@
     fw = sg + 4
     bw = 4 - sg
 
+    def got(like, sem):
+        pltpu.make_async_remote_copy(
+            src_ref=like, dst_ref=like, send_sem=rims.at[0], recv_sem=sem,
+            device_id=(ep ^ 1, y, x), device_id_type=MESH,
+        ).wait_recv()
+
+    def left(like, sem):
+        pltpu.make_async_remote_copy(
+            src_ref=like, dst_ref=like, send_sem=sem, recv_sem=rimr.at[0],
+            device_id=(ep ^ 1, y, x), device_id_type=MESH,
+        ).wait_send()
+
     def z_copy(u, cc):
         dest = ((z - unit_dz(u) + NZ) % NZ) * 2 + cc
         i, j = place(u)
         return pltpu.make_async_remote_copy(
-            src_ref=disp.at[dest], dst_ref=xg.at[u, i, j, core],
-            send_sem=zs.at[u, cc], recv_sem=zr.at[u, core],
+            src_ref=disp.at[dest], dst_ref=xg.at[u, 4 * i + j, core],
+            send_sem=zs.at[0], recv_sem=zr.at[u],
             device_id=(dest, y, x), device_id_type=MESH,
         )
 
-    def z_wait(u, c):
-        i, j = place(u)
-        pltpu.make_async_remote_copy(
-            src_ref=disp.at[0], dst_ref=xg.at[u, i, j, c],
-            send_sem=zs.at[u, c], recv_sem=zr.at[u, c],
-            device_id=(ep ^ 1, y, x), device_id_type=MESH,
-        ).wait_recv()
+    def z_wait(u):
+        i, j = place(u)
+
+        @pl.when(u != OWN)
+        def _():
+            got(xg.at[u, 4 * i + j], zr.at[u])
+
+        @pl.when(u == OWN)
+        def _():
+            got(xg.at[u, 4 * i + j, 1 - core], zr.at[u])
 
     def z_send(u, carry):
         for cc in (0, 1):
-            @pl.when(jnp.logical_not((u == 9) & (core == cc)))
+            @pl.when(jnp.logical_not((u == OWN) & (core == cc)))
             def _():
                 z_copy(u, cc).start()
         return carry
 
     lax.fori_loop(0, UNITS, z_send, 0)
-    xg[9, x, y, core] = disp[ep]
+    xg[OWN, 4 * x + y, core] = disp[ep]
 
     l_trig.wait()
     l_q.wait()
@@ -188,12 +194,12 @@
 
     def rotate_block(n, carry):
         rows = pl.ds(pl.multiple_of(n * WINDOW, WINDOW), WINDOW)
-        q = q_v[rows, :].astype(f32)
+        q = q_v[:, rows].astype(f32)
         k = k_v[rows, :].astype(f32)
         v = v_v[rows, :].astype(f32)
         k = jnp.where(group == 0, pltpu.roll(k, HD, 1), k)
         v = jnp.where(group == 0, pltpu.roll(v, HD, 1), v)
-        both = jnp.where(first, jnp.concatenate([q, q], axis=1), k)
+        both = jnp.where(first, jnp.concatenate([q, q], axis=0).T, k)
         block = ep * 4 + n
         cb = trig_v[2, pl.ds(block, 1), :]
         sb = trig_v[3, pl.ds(block, 1), :]
@@ -209,7 +215,7 @@
 
     lax.fori_loop(0, 4, rotate_block, 0)
     rim = pltpu.make_async_remote_copy(
-        src_ref=kv.at[4], dst_ref=kv.at[0], send_sem=ks.at[0], recv_sem=kr.at[0],
+        src_ref=kv.at[4], dst_ref=kv.at[0], send_sem=rims.at[0], recv_sem=rimr.at[0],
         device_id=((ep + 1) % 32, y, x), device_id_type=MESH,
     )
     rim.start()
@@ -242,22 +248,22 @@
 
     def attend(n):
         mixed = jnp.where(first, pltpu.roll(mix_of(n), HD, 1), mix_of(n + 2)).astype(bf16)
-        xg[UNITS + 2 * n, y, x] = mixed[:ROWS].reshape(2, SLOTS, 128)
-        xg[UNITS + 2 * n + 1, x, y] = mixed[ROWS:].reshape(2, SLOTS, 128)
+        xg[UNITS + 2 * n, 4 * y + x] = mixed[:ROWS].reshape(2, SLOTS, 128)
+        xg[UNITS + 2 * n + 1, 4 * x + y] = mixed[ROWS:].reshape(2, SLOTS, 128)
 
     def ag1_copy(u, k):
         i, j = place(u)
         return pltpu.make_async_remote_copy(
-            src_ref=xg.at[u, i, j], dst_ref=xg.at[u, i, j],
-            send_sem=a1s.at[u, k - 1], recv_sem=a1r.at[u, k - 1],
+            src_ref=xg.at[u, 4 * i + j], dst_ref=xg.at[u, 4 * i + j],
+            send_sem=ags.at[u], recv_sem=a1r.at[u],
             device_id=along_j(u, k), device_id_type=MESH,
         )
 
     def ag3_copy(u, side):
         i, j = place(u)
         return pltpu.make_async_remote_copy(
-            src_ref=xg.at[u, i], dst_ref=xg.at[u, i],
-            send_sem=a3s.at[u, side], recv_sem=a3r.at[u, side],
+            src_ref=xg.at[u, pl.ds(4 * i, 4)], dst_ref=xg.at[u, pl.ds(4 * i, 4)],
+            send_sem=ags.at[u], recv_sem=(a4r if side else a3r).at[u],
             device_id=along_i(u, bw if side else fw), device_id_type=MESH,
         )
 
@@ -265,28 +271,10 @@
         i, j = place(u)
         row = (i + bw) % 4
         return pltpu.make_async_remote_copy(
-            src_ref=xg.at[u, row], dst_ref=xg.at[u, row],
-            send_sem=a4s.at[u], recv_sem=a4r.at[u],
+            src_ref=xg.at[u, pl.ds(4 * row, 4)], dst_ref=xg.at[u, pl.ds(4 * row, 4)],
+            send_sem=ags.at[u], recv_sem=a4r.at[u],
             device_id=along_i(u, fw), device_id_type=MESH,
         )
-
-    def got(copy_like, dst, sem):
-        pltpu.make_async_remote_copy(
-            src_ref=dst, dst_ref=dst, send_sem=copy_like, recv_sem=sem,
-            device_id=(ep ^ 1, y, x), device_id_type=MESH,
-        ).wait_recv()
-
-    def ag1_got(u, k):
-        i, j = place(u)
-        got(a1s.at[u, k - 1], xg.at[u, i, (j + 4 - k) % 4], a1r.at[u, k - 1])
-
-    def ag3_got(u, side):
-        i, j = place(u)
-        got(a3s.at[u, side], xg.at[u, (i + (fw if side else bw)) % 4], a3r.at[u, side])
-
-    def ag4_got(u):
-        i, j = place(u)
-        got(a4s.at[u], xg.at[u, (i + 2) % 4], a4r.at[u])
 
     def gathered(u):
         odd = u % 2
@@ -295,7 +283,7 @@
             for xx in range(4):
                 a = jnp.where(odd == 1, xx, yy)
                 b = jnp.where(odd == 1, yy, xx)
-                tiles.append(xg[u, a, b].reshape(ROWS, 128))
+                tiles.append(xg[u, 4 * a + b].reshape(ROWS, 128))
         return jnp.concatenate(tiles, axis=1)
 
     def rs1_copy(u, side):
@@ -303,13 +291,13 @@
         dest = (j + (bw if side else 2)) % 4
         return pltpu.make_async_remote_copy(
             src_ref=yb.at[u, dest], dst_ref=(rb if side else ra).at[u],
-            send_sem=b1s.at[u, side], recv_sem=b1r.at[u, side],
+            send_sem=rss.at[u], recv_sem=(b2r if side else b1r).at[u],
             device_id=along_j(u, bw if side else fw), device_id_type=MESH,
         )
 
     def rs2_copy(u):
         return pltpu.make_async_remote_copy(
-            src_ref=tb.at[u], dst_ref=rc.at[u], send_sem=b2s.at[u], recv_sem=b2r.at[u],
+            src_ref=tb.at[u], dst_ref=rc.at[u], send_sem=rss.at[u], recv_sem=b2r.at[u],
             device_id=along_j(u, fw), device_id_type=MESH,
         )
 
@@ -317,7 +305,7 @@
         i, j = place(u)
         return pltpu.make_async_remote_copy(
             src_ref=qb.at[u, (i + k) % 4], dst_ref=rd.at[u, k - 1],
-            send_sem=b3s.at[u, k - 1], recv_sem=b3r.at[u, k - 1],
+            send_sem=rss.at[u], recv_sem=b3r.at[u],
             device_id=along_i(u, k), device_id_type=MESH,
         )
 
@@ -325,22 +313,22 @@
         dest = ((z + unit_dz(u) + NZ) % NZ) * 2 + cc
         return pltpu.make_async_remote_copy(
             src_ref=fb.at[u, cc], dst_ref=home.at[ep],
-            send_sem=hs.at[u, cc], recv_sem=hr.at[u, core],
+            send_sem=hs.at[0], recv_sem=hr.at[0],
             device_id=(dest, y, x), device_id_type=MESH,
         )
 
     def not_own(u, cc):
-        return jnp.logical_not((u == 9) & (core == cc))
+        return jnp.logical_not((u == OWN) & (core == cc))
 
     def tick(t, carry):
         u1 = t
 
-        @pl.when(t == 2)
+        @pl.when(t == ATTEND[0])
         def _():
             rim.wait_recv()
             attend(0)
 
-        @pl.when(t == 4)
+        @pl.when(t == ATTEND[1])
         def _():
             attend(1)
 
@@ -348,10 +336,7 @@
         def _():
             @pl.when(u1 < UNITS)
             def _():
-                for c in (0, 1):
-                    @pl.when(not_own(u1, c))
-                    def _():
-                        z_wait(u1, c)
+                z_wait(u1)
             for k in (1, 2, 3):
                 ag1_copy(u1, k).start()
 
@@ -360,8 +345,7 @@
         @pl.when((u2 >= 0) & (u2 < UNITS))
         def _():
             i, j = place(u2)
-            rs = rs1_copy(u2, 0)
-            rs.wait_recv()
+            got(ra.at[u2], b1r.at[u2])
             tb[u2] = (ra[u2].astype(f32) + yb[u2, (j + fw) % 4].astype(f32)).astype(bf16)
             rs2_copy(u2).start()
 
@@ -369,8 +353,7 @@
 
         @pl.when((u3 >= 0) & (u3 < ALL_UNITS))
         def _():
-            for k in (1, 2, 3):
-                ag1_got(u3, k)
+            got(xg.at[u3, pl.ds(0, 3)], a1r.at[u3])
             ag3_copy(u3, 0).start()
             ag3_copy(u3, 1).start()
 
@@ -378,7 +361,7 @@
 
         @pl.when((u4 >= 0) & (u4 < ALL_UNITS))
         def _():
-            ag3_got(u4, 0)
+            got(xg.at[u4, pl.ds(0, 4)], a3r.at[u4])
             ag4_copy(u4).start()
 
         u5 = t - RS3
@@ -386,8 +369,7 @@
         @pl.when((u5 >= 0) & (u5 < UNITS))
         def _():
             i, j = place(u5)
-            rs1_copy(u5, 1).wait_recv()
-            rs2_copy(u5).wait_recv()
+            got(xg.at[u5, pl.ds(0, 8)], b2r.at[u5])
             qb[u5] = (yb[u5, j].astype(f32) + rc[u5].astype(f32) + rb[u5].astype(f32)).astype(bf16)
             for k in (1, 2, 3):
                 rs3_copy(u5, k).start()
@@ -397,8 +379,7 @@
         @pl.when((u6 >= 0) & (u6 < UNITS))
         def _():
             i, j = place(u6)
-            for k in (1, 2, 3):
-                rs3_copy(u6, k).wait_recv()
+            got(rd.at[u6], b3r.at[u6])
             total = qb[u6, i].astype(f32) + rd[u6, 0].astype(f32) + rd[u6, 1].astype(f32) + rd[u6, 2].astype(f32)
             fb[u6] = total.astype(bf16).reshape(2, SLOTS, 128)
             for cc in (0, 1):
@@ -420,8 +401,7 @@
 
         @pl.when((um >= 0) & (um < ALL_UNITS))
         def _():
-            ag3_got(um, 1)
-            ag4_got(um)
+            got(xg.at[um, pl.ds(0, 8)], a4r.at[um])
 
         @pl.when((um >= 0) & (um < UNITS))
         def _():
@@ -449,49 +429,36 @@
 
         @pl.when((u6 >= 0) & (u6 < ALL_UNITS))
         def _():
-            for k in (1, 2, 3):
-                ag1_copy(u6, k).wait_send()
-            ag3_copy(u6, 0).wait_send()
-            ag3_copy(u6, 1).wait_send()
-            ag4_copy(u6).wait_send()
+            left(xg.at[u6, pl.ds(0, 15)], ags.at[u6])
 
         @pl.when((u6 >= 0) & (u6 < UNITS))
         def _():
-            for cc in (0, 1):
-                @pl.when(not_own(u6, cc))
-                def _():
-                    z_copy(u6, cc).wait_send()
-            rs1_copy(u6, 0).wait_send()
-            rs1_copy(u6, 1).wait_send()
-            rs2_copy(u6).wait_send()
-            for k in (1, 2, 3):
-                rs3_copy(u6, k).wait_send()
+            left(xg.at[u6, pl.ds(0, 15)], rss.at[u6])
 
         return carry
 
     lax.fori_loop(0, ALL_UNITS + FIN, tick, 0)
 
     l_rw.wait()
-    weights = rw_v[...]
-    slot0 = jnp.sum(one0 * (rank + e_iota.astype(f32) * float(SLOTS)), axis=1, keepdims=True)
-    slot1 = jnp.sum(one1 * (rank + e_iota.astype(f32) * float(SLOTS)), axis=1, keepdims=True)
+    eye = t_col == t_row
+
+    def as_column(row):
+        return jnp.sum(jnp.where(eye, row, 0.0), axis=1, keepdims=True)
+
+    weight0 = as_column(rw_v[0:1, :])
+    weight1 = as_column(rw_v[1:2, :])
+    slot0 = as_column(slot_row0)
+    slot1 = as_column(slot_row1)
     slot_lane = lax.broadcasted_iota(jnp.int32, (TOK_E, EXPERTS * SLOTS), 1).astype(f32)
     pick0 = (slot_lane == slot0).astype(f32).astype(bf16)
     pick1 = (slot_lane == slot1).astype(f32).astype(bf16)
 
-    def arrived(u, carry):
-        for c in (0, 1):
-            @pl.when(not_own(u, c))
-            def _():
-                src = ((z - unit_dz(u) + NZ) % NZ) * 2 + c
-                got(hs.at[u, c], home.at[src], hr.at[u, c])
-                home_copy(u, c).wait_send()
-        return carry
-
-    lax.fori_loop(0, UNITS, arrived, 0)
+    got(home.at[pl.ds(0, EXPERTS - 1)], hr.at[0])
+    left(home.at[pl.ds(0, EXPERTS - 1)], hs.at[0])
+    left(disp.at[pl.ds(0, EXPERTS - 1)], zs.at[0])
     rim.wait_send()
     results = home[...].reshape(EXPERTS * SLOTS, 128)
-    combined = dot(pick0, results) * weights[:, 0:1] + dot(pick1, results) * weights[:, 1:2]
+    combined = dot(pick0, results) * weight0 + dot(pick1, results) * weight1
     eout_ref[...] = combined.astype(bf16)
 
 
@@ -523,14 +490,14 @@
         in_specs=[any_spec] * 3 + [smem] + [any_spec] * 9,
         out_specs=(vmem, vmem),
         scratch_shapes=[
-            pltpu.VMEM((TOK_A, HD), bf16),
+            pltpu.VMEM((HD, TOK_A), bf16),
             pltpu.VMEM((TOK_A, 128), bf16),
             pltpu.VMEM((TOK_A, 128), bf16),
             pltpu.VMEM((HEADS * HD, 128), bf16),
             pltpu.VMEM((TOK_E, D), bf16),
             pltpu.VMEM((1, D), f32),
-            pltpu.VMEM((TOK_E, 2), jnp.int32),
-            pltpu.VMEM((TOK_E, 2), f32),
+            pltpu.VMEM((2, TOK_E), jnp.int32),
+            pltpu.VMEM((2, TOK_E), f32),
             pltpu.VMEM((D, FF_HERE), bf16),
             pltpu.VMEM((D, FF_HERE), bf16),
             pltpu.VMEM((FF_HERE, D), bf16),
@@ -540,7 +507,7 @@
             pltpu.VMEM((D, 256), bf16),
             pltpu.VMEM((4, WINDOW, 128), bf16),
             pltpu.VMEM((5, WINDOW, 128), bf16),
-            pltpu.VMEM((ALL_UNITS, 4, 4, 2, SLOTS, 128), bf16),
+            pltpu.VMEM((ALL_UNITS, 16, 2, SLOTS, 128), bf16),
             pltpu.VMEM((UNITS, 4, 4, ROWS, 128), bf16),
             pltpu.VMEM((UNITS, 4, ROWS, 128), bf16),
             pltpu.VMEM((UNITS, 4, ROWS, 128), bf16),
@@ -551,22 +518,18 @@
             pltpu.VMEM((UNITS, 2, SLOTS, 128), bf16),
             pltpu.VMEM((EXPERTS, SLOTS, 128), bf16),
             dma((12,)),
-            dma((UNITS, 2)),
-            dma((UNITS, 2)),
-            dma((UNITS, 2)),
-            dma((UNITS, 2)),
-            dma((ALL_UNITS, 3)),
-            dma((ALL_UNITS, 3)),
-            dma((ALL_UNITS, 2)),
-            dma((ALL_UNITS, 2)),
+            dma((1,)),
+            dma((UNITS,)),
+            dma((1,)),
+            dma((1,)),
             dma((ALL_UNITS,)),
             dma((ALL_UNITS,)),
-            dma((UNITS, 2)),
-            dma((UNITS, 2)),
+            dma((ALL_UNITS,)),
+            dma((ALL_UNITS,)),
             dma((UNITS,)),
             dma((UNITS,)),
-            dma((UNITS, 3)),
-            dma((UNITS, 3)),
+            dma((UNITS,)),
+            dma((UNITS,)),
             dma((1,)),
             dma((1,)),
         ],
@@ -574,7 +537,7 @@
             collective_id=0, has_side_effects=True, vmem_limit_bytes=60 * 1024 * 1024
         ),
     )(
-        queries, keys, values, sink_logits, out_weight, expert_input, norm_gain.reshape(1, D), routes, route_weights,
+        queries.T, keys, values, sink_logits, out_weight, expert_input, norm_gain.reshape(1, D), routes.T, route_weights.T,
         gate_weight[0], up_weight[0], down_weight[0], trig,
     )
 

time: 109 us -> 94.7 us (0.87)
  Pallas kernels: 102 us -> 91 us
  local copies, waits for them, and re-layouts: 5.41 us -> 2.23 us
    pallas_call x1, Pallas kernels: 102 us -> 91 us  [local(): pl.pallas_call(kernel, out_shape=(jax.ShapeDtypeStruct((TOK_A, 128), bf16...]
    unnamed x11 -> x4, local copies, waits for them, and re-layouts: 5.41 us -> 2.23 us
where the time goes in v2:
time: 94.7 us; the launch traced here: 94.5 us
  Pallas kernels  91 us (96%)
  local copies, waits for them, and re-layouts  2.23 us (2%)
  between operations  1.3 us (1%)
    pallas_call x1, Pallas kernels, local(): pl.pallas_call(kernel, out_shape=(jax.ShapeDtypeStruct((TOK_A, 128), bf16...  91 us
    unnamed x4, local copies, waits for them, and re-layouts  2.23 us

profile of v2, /device:TPU:1, one launch (start us, length us, event | category | flops | bytes accessed | tf_op | source)
XLA Modules:
  0.0 94.5 jit_solution(6596620455807469180)
XLA Ops:
  1.3 91.0 %shard_map.140 = (bf16[512,128]{1,0:T(8,128)(2,1)}, bf16[256,128]{1,0:T(8,128)(2,1)}) custom-call(bf16[64,512]{1,0:T(8,128)(2,1)} %bitcast.10, bf16[512,128]{1,0:T(8,128)(2,1)} %k_in.1, bf16[512,128]{1,0:T(8,128)(2,1)} %v_in.1, f32[1]{0:T(128)S(6)} %copy.17.sink_ref, bf16[1024,128]{1,0:T(8,128)(2,1)} %ow_in.1, bf16[256,2048]{1,0:T(8,128)(2,1)} %x_in.1, ...), custom_call_target="tpu_custom_call" | custom-call | tf_op jit(solution)/shard_map/pallas_call | solution.py:484
  92.3 0.0 copy-start
  92.3 1.6 %copy.18 = bf16[512,128]{1,0:T(8,128)(2,1)} copy(bf16[512,128]{1,0:T(8,128)(2,1)} %get-tuple-element.4) | data formatting | bytes 262144
  93.9 0.0 copy-done
  93.9 0.6 copy.19
Async XLA Ops:
  92.3 1.6 %copy-start = (bf16[256,128]{1,0:T(8,128)(2,1)S(1)}, bf16[256,128]{1,0:T(8,128)(2,1)}, u32[]{:S(2)}) copy-start(bf16[256,128]{1,0:T(8,128)(2,1)} %get-tuple-element.5) | copy-start | bytes 196612

commit v3 on v2

--- a/solution.py
+++ b/solution.py
@@ -25,9 +25,10 @@
 TOK_A = 512
 MESH = pl.DeviceIdType.MESH
 OWN = 15
+LEAD = 5
 ATTEND = (8, 10)
 
-AG3, AG4, MM, RS2, RS3, FIN = 2, 4, 6, 8, 10, 12
+AG3, AG4, MM, RS2, RS3, FIN = 3, 6, 9, 12, 15, 18
 
 rms_eps = 1e-06
 mask_value = -1e30
@@ -37,10 +38,10 @@
 
 
 def unit_dz(u):
-    late = u - 7
-    out = jnp.where(u == 6, 8, (2 + 2 * (u // 2)) * (1 - 2 * (u % 2)))
-    back = jnp.where(u == OWN, 0, (7 - 2 * (late // 2)) * (1 - 2 * (late % 2)))
-    return jnp.where(u < 7, out, back)
+    sign = 1 - 2 * (u % 2)
+    out = jnp.where(u == 10, 8, (2 + u // 2) * sign)
+    back = jnp.where(u == OWN, 0, jnp.where(u < 13, -7 * sign, -1 * sign))
+    return jnp.where(u < 11, out, back)
 
 
 def rope_tables():
@@ -61,7 +62,7 @@
     q_in, k_in, v_in, sink_ref, ow_in, x_in, gain_in, routes_in, rw_in, wg_in, wu_in, wd_in, trig_in,
     attn_ref, eout_ref,
     q_v, k_v, v_v, ow_v, x_v, gain_v, routes_v, rw_v, wg_v, wu_v, wd_v, trig_v,
-    nrm, disp, w01, qp, kv, xg, yb, ra, rb, rc, tb, qb, rd, fb, home,
+    disp, w01, qp, kv, xg, yb, ra, rb, rc, tb, qb, rd, fb, home,
     in_sem, zs, zr, hs, hr, ags, a1r, a3r, a4r, rss, b1r, b2r, b3r, rims, rimr,
 ):
     ep = lax.axis_index("ep")
@@ -72,6 +73,14 @@
     tp = y * 4 + x
     sg = 1 - 2 * core
 
+    barrier = pltpu.get_barrier_semaphore()
+
+    for step in sorted(range(1, 32), key=lambda n: -min(n, 32 - n)):
+        pl.semaphore_signal(barrier, inc=1, device_id=((ep + step) % 32, y, x), device_id_type=MESH)
+    for k in (1, 2, 3):
+        pl.semaphore_signal(barrier, inc=1, device_id=(ep, (y + k) % 4, x), device_id_type=MESH)
+        pl.semaphore_signal(barrier, inc=1, device_id=(ep, y, (x + k) % 4), device_id_type=MESH)
+
     pairs = [
         (routes_in, routes_v), (x_in, x_v), (gain_in, gain_v), (rw_in, rw_v), (trig_in, trig_v), (q_in, q_v),
         (k_in, k_v), (v_in, v_v), (wg_in, wg_v), (wu_in, wu_v), (wd_in, wd_v), (ow_in, ow_v),
@@ -80,17 +89,6 @@
     for load in loads:
         load.start()
     (l_routes, l_x, l_gain, l_rw, l_trig, l_q, l_k, l_v, l_wg, l_wu, l_wd, l_ow) = loads
-
-    barrier = pltpu.get_barrier_semaphore()
-
-    def hello(step, carry):
-        pl.semaphore_signal(barrier, inc=1, device_id=((ep + step) % 32, y, x), device_id_type=MESH)
-        return carry
-
-    lax.fori_loop(1, 32, hello, 0)
-    for k in (1, 2, 3):
-        pl.semaphore_signal(barrier, inc=1, device_id=(ep, (y + k) % 4, x), device_id_type=MESH)
-        pl.semaphore_signal(barrier, inc=1, device_id=(ep, y, (x + k) % 4), device_id_type=MESH)
 
     l_routes.wait()
     e_iota = lax.broadcasted_iota(jnp.int32, (EXPERTS, TOK_E), 0)
@@ -108,15 +106,12 @@
     own_cols = pl.ds(pl.multiple_of(tp * 128, 128), 128)
     gain = gain_v[:, own_cols]
 
-    def norm_rows(n, carry):
-        rows = pl.ds(pl.multiple_of(n * 32, 32), 32)
-        wide = x_v[rows, :].astype(f32)
-        inv = lax.rsqrt(jnp.mean(wide * wide, axis=1, keepdims=True) + rms_eps)
-        nrm[rows, :] = (x_v[rows, own_cols].astype(f32) * inv * gain).astype(bf16)
-        return carry
-
-    lax.fori_loop(0, 8, norm_rows, 0)
-    normed = nrm[...]
+    squares = jnp.zeros((TOK_E, 128), f32)
+    for n in range(D // 128):
+        wide = x_v[:, n * 128:(n + 1) * 128].astype(f32)
+        squares = squares + wide * wide
+    inv = lax.rsqrt(jnp.sum(squares, axis=1, keepdims=True) * (1.0 / D) + rms_eps)
+    normed = (x_v[:, own_cols].astype(f32) * inv * gain).astype(bf16)
 
     def fill_slots(n, carry):
         slot = (lax.broadcasted_iota(jnp.int32, (256, TOK_E), 0) + n * 256).astype(f32)
@@ -181,7 +176,7 @@
                 z_copy(u, cc).start()
         return carry
 
-    lax.fori_loop(0, UNITS, z_send, 0)
+    lax.fori_loop(0, LEAD, z_send, 0)
     xg[OWN, 4 * x + y, core] = disp[ep]
 
     l_trig.wait()
@@ -331,6 +326,10 @@
         @pl.when(t == ATTEND[1])
         def _():
             attend(1)
+
+        @pl.when(t + LEAD < UNITS)
+        def _():
+            z_send(t + LEAD, 0)
 
         @pl.when(u1 < ALL_UNITS)
         def _():
@@ -484,8 +483,8 @@
     return pl.pallas_call(
         kernel,
         out_shape=(
-            jax.ShapeDtypeStruct((TOK_A, 128), bf16),
-            jax.ShapeDtypeStruct((TOK_E, 128), bf16),
+            pltpu.VMEM((TOK_A, 128), bf16),
+            pltpu.VMEM((TOK_E, 128), bf16),
         ),
         in_specs=[any_spec] * 3 + [smem] + [any_spec] * 9,
         out_specs=(vmem, vmem),
@@ -502,7 +501,6 @@
             pltpu.VMEM((D, FF_HERE), bf16),
             pltpu.VMEM((FF_HERE, D), bf16),
             pltpu.VMEM((4, 128, 128), f32),
-            pltpu.VMEM((TOK_E, 128), bf16),
             pltpu.VMEM((EXPERTS, SLOTS, 128), bf16),
             pltpu.VMEM((D, 256), bf16),
             pltpu.VMEM((4, WINDOW, 128), bf16),
@@ -534,7 +532,7 @@
             dma((1,)),
         ],
         compiler_params=pltpu.CompilerParams(
-            collective_id=0, has_side_effects=True, vmem_limit_bytes=60 * 1024 * 1024
+            collective_id=0, has_side_effects=True, vmem_limit_bytes=63 * 1024 * 1024 + 512 * 1024
         ),
     )(
         queries.T, keys, values, sink_logits, out_weight, expert_input, norm_gain.reshape(1, D), routes.T, route_weights.T,

time: 94.7 us -> 89.6 us (0.946)
  Pallas kernels: 91 us -> 86.9 us
    pallas_call x1, Pallas kernels: 91 us -> 86.9 us  [local(): pl.pallas_call(kernel, out_shape=(pltpu.VMEM((TOK_A, 128), bf16), pltpu.V...]
    unnamed x4 -> x2, local copies, waits for them, and re-layouts: 2.23 us -> 1.29 us
where the time goes in v3:
time: 89.6 us; the launch traced here: 89.4 us
  Pallas kernels  86.9 us (97%)
  local copies, waits for them, and re-layouts  1.29 us (1%)
  between operations  1.29 us (1%)
    pallas_call x1, Pallas kernels, local(): pl.pallas_call(kernel, out_shape=(pltpu.VMEM((TOK_A, 128), bf16), pltpu.V...  86.9 us

profile of v3, /device:TPU:1, one launch (start us, length us, event | category | flops | bytes accessed | tf_op | source)
XLA Modules:
  0.0 89.4 jit_solution(1804220597858857258)
XLA Ops:
  1.3 86.9 %shard_map.140 = (bf16[512,128]{1,0:T(8,128)(2,1)S(1)}, bf16[256,128]{1,0:T(8,128)(2,1)S(1)}) custom-call(bf16[64,512]{1,0:T(8,128)(2,1)} %bitcast.10, bf16[512,128]{1,0:T(8,128)(2,1)} %k_in.1, bf16[512,128]{1,0:T(8,128)(2,1)} %v_in.1, f32[1]{0:T(128)S(6)} %copy.19.sink_ref, bf16[1024,128]{1,0:T(8,128)(2,1)} %ow_in.1, bf16[256,2048]{1,0:T(8,128)(2,1)} %x_in.1, ...), custom_call_target="tpu_custom_call" | custom-call | tf_op jit(solution)/shard_map/pallas_call | solution.py:483
  88.2 0.7 copy.17
  88.8 0.6 copy.18

commit v4 on v3

--- a/solution.py
+++ b/solution.py
@@ -26,7 +26,7 @@
 MESH = pl.DeviceIdType.MESH
 OWN = 15
 LEAD = 5
-ATTEND = (8, 10)
+ATTEND = (11, 13)
 
 AG3, AG4, MM, RS2, RS3, FIN = 3, 6, 9, 12, 15, 18
 
@@ -122,16 +122,16 @@
     lax.fori_loop(0, 4, fill_slots, 0)
     pl.semaphore_wait(barrier, 37)
 
-    def place(u):
-        odd = u % 2
+    def place(u, of=core):
+        odd = (u + of) % 2
         return jnp.where(odd == 1, x, y), jnp.where(odd == 1, y, x)
 
     def along_j(u, k):
-        odd = u % 2
+        odd = (u + core) % 2
         return (ep, jnp.where(odd == 1, (y + k) % 4, y), jnp.where(odd == 1, x, (x + k) % 4))
 
     def along_i(u, k):
-        odd = u % 2
+        odd = (u + core) % 2
         return (ep, jnp.where(odd == 1, y, (y + k) % 4), jnp.where(odd == 1, (x + k) % 4, x))
 
     fw = sg + 4
@@ -151,7 +151,7 @@
 
     def z_copy(u, cc):
         dest = ((z - unit_dz(u) + NZ) % NZ) * 2 + cc
-        i, j = place(u)
+        i, j = place(u, cc)
         return pltpu.make_async_remote_copy(
             src_ref=disp.at[dest], dst_ref=xg.at[u, 4 * i + j, core],
             send_sem=zs.at[0], recv_sem=zr.at[u],
@@ -177,7 +177,8 @@
         return carry
 
     lax.fori_loop(0, LEAD, z_send, 0)
-    xg[OWN, 4 * x + y, core] = disp[ep]
+    own_i, own_j = place(OWN)
+    xg[OWN, 4 * own_i + own_j, core] = disp[ep]
 
     l_trig.wait()
     l_q.wait()
@@ -243,8 +244,9 @@
 
     def attend(n):
         mixed = jnp.where(first, pltpu.roll(mix_of(n), HD, 1), mix_of(n + 2)).astype(bf16)
-        xg[UNITS + 2 * n, 4 * y + x] = mixed[:ROWS].reshape(2, SLOTS, 128)
-        xg[UNITS + 2 * n + 1, 4 * x + y] = mixed[ROWS:].reshape(2, SLOTS, 128)
+        i, j = place(0)
+        xg[UNITS + 2 * n, 4 * i + j] = mixed[:ROWS].reshape(2, SLOTS, 128)
+        xg[UNITS + 2 * n + 1, 4 * j + i] = mixed[ROWS:].reshape(2, SLOTS, 128)
 
     def ag1_copy(u, k):
         i, j = place(u)
@@ -272,7 +274,7 @@
         )
 
     def gathered(u):
-        odd = u % 2
+        odd = (u + core) % 2
         tiles = []
         for yy in range(4):
             for xx in range(4):
@@ -405,7 +407,7 @@
         @pl.when((um >= 0) & (um < UNITS))
         def _():
             i, j = place(um)
-            odd = um % 2
+            odd = (um + core) % 2
             rows_in = gathered(um)
             gate = dot(rows_in, wg_v[...])
             up = dot(rows_in, wu_v[...])

time: 89.6 us -> 88.7 us (0.990)
  Pallas kernels: 86.9 us -> 86 us
where the time goes in v4:
time: 88.7 us; the launch traced here: 88.6 us
  Pallas kernels  86 us (97%)
  local copies, waits for them, and re-layouts  1.29 us (1%)
  between operations  1.29 us (1%)
    pallas_call x1, Pallas kernels, local(): pl.pallas_call(kernel, out_shape=(pltpu.VMEM((TOK_A, 128), bf16), pltpu.V...  86 us

profile of v4, /device:TPU:1, one launch (start us, length us, event | category | flops | bytes accessed | tf_op | source)
XLA Modules:
  0.0 88.6 jit_solution(511796674456816192)
XLA Ops:
  1.3 86.0 %shard_map.140 = (bf16[512,128]{1,0:T(8,128)(2,1)S(1)}, bf16[256,128]{1,0:T(8,128)(2,1)S(1)}) custom-call(bf16[64,512]{1,0:T(8,128)(2,1)} %bitcast.10, bf16[512,128]{1,0:T(8,128)(2,1)} %k_in.1, bf16[512,128]{1,0:T(8,128)(2,1)} %v_in.1, f32[1]{0:T(128)S(6)} %copy.19.sink_ref, bf16[1024,128]{1,0:T(8,128)(2,1)} %ow_in.1, bf16[256,2048]{1,0:T(8,128)(2,1)} %x_in.1, ...), custom_call_target="tpu_custom_call" | custom-call | tf_op jit(solution)/shard_map/pallas_call | solution.py:485
  87.3 0.7 copy.17
  87.9 0.6 copy.18
